TPU v7x, 32 devices: a whole 2x2x4 slice. The times are simulated.
32 devices in a mesh: rep: 2 (over x), fs: 8 (over z, y), tp: 2 (over core).
Axes of the slice: x: 2, y: 2, z: 4, core: 2. Of those that a mesh axis runs over, the one named last changes fastest.
Arguments:
- resid: bfloat16 [16384, 2048], P(('rep', 'fs'), 'tp'), may hold values from -6 to 6
- gain_mix_in: float32 [2048], replicated, may hold values from 0.1 to 1.9
- u_weight: float32 [2048, 1024], P('fs', 'tp'), may hold values from -0.125 to 0.125
- v_weight: float32 [2048, 1024], P('fs', 'tp'), may hold values from -0.125 to 0.125
- u_scale: float32 [1024], P('tp'), may hold values from 0.5 to 2
- v_scale: float32 [1024], P('tp'), may hold values from 0.3 to 3
- v_gain: float32 [1024], P('tp'), may hold values from 0.1 to 1.9
- mix_matrix: float32 [16, 128, 128], P('tp'), may hold values from -0.5 to 0.5
- mix_bias: float32 [16, 128], P('tp'), may hold values from 0.1 to 1.9
- out_weight: float32 [1024, 2048], P('tp', 'fs'), may hold values from -0.1875 to 0.1875
- out_scale: float32 [2048], P('fs'), may hold values from 0.3 to 3
- gain_mix_out: float32 [2048], replicated, may hold values from 0.1 to 1.9
- gain_ffn_in: float32 [2048], replicated, may hold values from 0.1 to 1.9
- up_weight: float32 [2048, 4096], P('fs', 'tp'), may hold values from -0.125 to 0.125
- up_scale: float32 [4096], P('tp'), may hold values from 0.5 to 2
- down_weight: float32 [4096, 2048], P('tp', 'fs'), may hold values from -0.09375 to 0.09375
- down_scale: float32 [2048], P('fs'), may hold values from 0.3 to 3
- gain_ffn_out: float32 [2048], replicated, may hold values from 0.1 to 1.9
Outputs:
- result: bfloat16 [16384, 2048], P(('rep', 'fs'), 'tp')
All inputs are finite; a program needn't handle non-finite values.
Results may differ from a plain program's by a relative error of at most 0.013.
Values may be sent and summed in bfloat16 or wider, within the bound.
A program may use at most 128 MiB of HBM per device.

v0:
```python
import jax
import jax.numpy as jnp
from jax import lax
from jax.sharding import PartitionSpec as P


def rms_norm(values, gain, width, power_sum):
    return values * lax.rsqrt(power_sum / width + 1e-06) * gain


def local(
    resid,
    gain_mix_in,
    u_weight,
    v_weight,
    u_scale,
    v_scale,
    v_gain,
    mix_matrix,
    mix_bias,
    out_weight,
    out_scale,
    gain_mix_out,
    gain_ffn_in,
    up_weight,
    up_scale,
    down_weight,
    down_scale,
    gain_ffn_out,
):
    rows = resid.shape[0]
    part_width = resid.shape[1]
    width = part_width * lax.axis_size("tp")
    lane = lax.axis_index("tp")
    full_rows = lax.all_gather(resid, "tp", axis=1, tiled=True)
    out_scales, down_scales = (
        lax.all_gather(out_scale, "fs", axis=0, tiled=True),
        lax.all_gather(down_scale, "fs", axis=0, tiled=True),
    )
    full_float = full_rows.astype(jnp.float32)
    normed = rms_norm(
        full_float, gain_mix_in, width, jnp.sum(full_float * full_float, axis=1, keepdims=True)
    ).astype(jnp.bfloat16)
    branch_cols = u_weight.shape[1]
    u_pre = jnp.dot(
        normed,
        lax.all_gather(u_weight.astype(jnp.bfloat16), "fs", axis=0, tiled=True),
        preferred_element_type=jnp.float32,
    )
    v_pre = jnp.dot(
        normed,
        lax.all_gather(v_weight.astype(jnp.bfloat16), "fs", axis=0, tiled=True),
        preferred_element_type=jnp.float32,
    )
    u_act = jax.nn.gelu(u_pre * u_scale)
    v_act = jax.nn.gelu(v_pre * v_scale)
    total, squares = lax.psum(
        (jnp.sum(v_act, axis=1, keepdims=True), jnp.sum(v_act * v_act, axis=1, keepdims=True)), "tp"
    )
    branch_width = branch_cols * lax.axis_size("tp")
    centre = total / branch_width
    spread = squares / branch_width - centre * centre
    v_norm = ((v_act - centre) * lax.rsqrt(spread + 1e-06) * v_gain).astype(jnp.bfloat16)
    groups = mix_matrix.shape[0]
    block = mix_matrix.shape[1]
    blocks = v_norm.reshape(rows // block, block, groups, branch_cols // groups)
    mixed = (
        jnp.einsum(
            "gts,bsgd->btgd",
            mix_matrix.astype(jnp.bfloat16),
            blocks,
            preferred_element_type=jnp.float32,
        )
        + mix_bias.T[None, :, :, None]
    )
    gated = (u_act * mixed.reshape(rows, branch_cols)).astype(jnp.bfloat16)
    partial_value = jnp.dot(
        gated,
        lax.all_gather(out_weight.astype(jnp.bfloat16), "fs", axis=1, tiled=True),
        preferred_element_type=jnp.float32,
    )
    mix_out = lax.psum(partial_value.astype(jnp.bfloat16), "tp").astype(jnp.float32) * out_scales
    power = jnp.sum(mix_out * mix_out, axis=1, keepdims=True)
    middle_full = (full_float + rms_norm(mix_out, gain_mix_out, width, power)).astype(jnp.bfloat16)
    middle = lax.dynamic_slice_in_dim(middle_full, lane * part_width, part_width, 1)
    middle_float = middle_full.astype(jnp.float32)
    ffn_in = rms_norm(
        middle_float,
        gain_ffn_in,
        width,
        jnp.sum(middle_float * middle_float, axis=1, keepdims=True),
    ).astype(jnp.bfloat16)
    up_half = up_weight.astype(jnp.bfloat16)
    down_half = down_weight.astype(jnp.bfloat16)
    whole_up = lax.all_gather(up_half, "fs", axis=0, tiled=True)
    raised = jnp.dot(ffn_in, whole_up, preferred_element_type=jnp.float32)
    hidden = jnp.square(jax.nn.relu(raised * up_scale)).astype(jnp.bfloat16)
    whole_down = lax.all_gather(down_half, "fs", axis=1, tiled=True)
    terms = jnp.dot(hidden, whole_down, preferred_element_type=jnp.float32)
    own_down = lax.dynamic_slice_in_dim(down_scales, lane * part_width, part_width, 0)
    ffn_out = (
        lax.psum_scatter(terms.astype(jnp.bfloat16), "tp", scatter_dimension=1, tiled=True).astype(
            jnp.float32
        )
        * own_down
    )
    power_out = lax.psum(jnp.sum(ffn_out * ffn_out, axis=1, keepdims=True), "tp")
    own_gain_out = lax.dynamic_slice_in_dim(gain_ffn_out, lane * part_width, part_width, 0)
    return (middle.astype(jnp.float32) + rms_norm(ffn_out, own_gain_out, width, power_out)).astype(
        jnp.bfloat16
    )


def solution(mesh):
    in_specs = (
        P(("rep", "fs"), "tp"),
        P(),
        P("fs", "tp"),
        P("fs", "tp"),
        P("tp"),
        P("tp"),
        P("tp"),
        P("tp", None, None),
        P("tp", None),
        P("tp", "fs"),
        P("fs"),
        P(),
        P(),
        P("fs", "tp"),
        P("tp"),
        P("tp", "fs"),
        P("fs"),
        P(),
    )
    out_specs = P(("rep", "fs"), "tp")
    return jax.shard_map(local, mesh=mesh, in_specs=in_specs, out_specs=out_specs, check_vma=False)
```

profile of v0, /device:TPU:0, one launch (start us, length us, event | category | flops | bytes accessed | tf_op | source)
XLA Modules:
  0.0 528.2 jit_solution(6334842264117924044)
XLA Ops:
  11.8 13.5 %all-gather.9.cloned.1.call-done = bf16[1024,2048]{1,0:T(8,128)(2,1)} async-done(((bf16[1024,1024]{1,0:T(8,128)(2,1)}), bf16[1024,2048]{1,0:T(8,128)(2,1)}) %all-gather.9.cloned.1.call-update) | async-done | bytes 4194320 | tf_op jit(solution)/shard_map/all_gather | solution.py:35
  25.3 3.1 fusion.3
  28.4 49.3 %all-gather.13.cloned.1.call-done = bf16[2048,512]{1,0:T(8,128)(2,1)} async-done(((bf16[256,512]{1,0:T(8,128)(2,1)}), bf16[2048,512]{1,0:T(8,128)(2,1)}) %all-gather.13.cloned.1.call-update) | async-done | bytes 2097168 | tf_op jit(solution)/shard_map/all_gather | solution.py:52
  77.7 5.8 %fusion.50 = (f32[1024]{0:T(1024)S(1)}, f32[1024]{0:T(1024)S(1)}, f32[1024,512]{1,0:T(8,128)S(1)}) fusion(f32[512]{0:T(512)S(1)} %copy-done.12, bf16[2048,512]{1,0:T(8,128)(2,1)} %all-gather.13.cloned.1.call-done, bf16[1024,2048]{1,0:T(8,128)(2,1)} %all-gather.9.cloned.1.call-done, f32[2048]{0:T(1024)S(1)} %copy-done.9, f32[1024]{0:T(1024)S(1)} %add_rsqrt_fusion.4), kind=kOutput, calls=%fused_computation.61 | convolution fusion | flops 2162161664 | bytes 8411136 | tf_op jit(solution)/shard_map/dot_general | solution.py:50
  83.5 2.5 all-reduce
  86.4 2.1 reshape.48
  88.5 2.4 bitcast_add_fusion
  90.9 2.7 copy.36
  93.6 3.4 reshape.49
  97.1 30.4 %all-gather.11.cloned.1.call-done = bf16[2048,512]{1,0:T(8,128)(2,1)} async-done(((bf16[256,512]{1,0:T(8,128)(2,1)}), bf16[2048,512]{1,0:T(8,128)(2,1)}) %all-gather.11.cloned.1.call-update) | async-done | bytes 2097168 | tf_op jit(solution)/shard_map/all_gather | solution.py:47
  127.5 50.8 %all-gather.15.cloned.1.call-done = bf16[512,2048]{1,0:T(8,128)(2,1)} async-done(((bf16[512,256]{1,0:T(8,128)(2,1)}), bf16[512,2048]{1,0:T(8,128)(2,1)}) %all-gather.15.cloned.1.call-update) | async-done | bytes 2097168 | tf_op jit(solution)/shard_map/all_gather | solution.py:79
  178.3 10.4 %convolution_convert_fusion = bf16[1024,2048]{1,0:T(8,128)(2,1)} fusion(bf16[512,2048]{1,0:T(8,128)(2,1)} %all-gather.15.cloned.1.call-done, f32[1024,512]{1,0:T(8,128)S(1)} %reshape.49, bf16[2048,512]{1,0:T(8,128)(2,1)} %all-gather.11.cloned.1.call-done, bf16[1024,2048]{1,0:T(8,128)(2,1)} %all-gather.9.cloned.1.call-done, f32[2048]{0:T(1024)S(1)} %copy-done.9, ...), kind=kOutput, calls=%fused_computation.23 | convolution fusion | flops 4311220224 | bytes 14694400 | tf_op jit(solution)/shard_map/dot_general | solution.py:77
  191.6 2.9 convert_element_type.76
  194.5 17.7 %all-gather = f32[8,1,256]{2,1,0:T(1,128)S(1)} all-gather(f32[1,1,256]{2,1,0:T(1,128)S(1)} %bitcast.35), channel_id=1, replica_groups=mesh['rep'=2,'fs'=8,'tp'=2] {'fs'}, dimensions={0}, use_global_device_ids=true | all-gather | bytes 9216 | tf_op jit(solution)/shard_map/all_gather | solution.py:37
  212.2 3.0 all-reduce.3.cloned.1.call-done
  215.3 3.5 multiply_reduce_fusion
  218.8 5.6 %fusion = (f32[1024]{0:T(1024)S(1)}, bf16[1024,2048]{1,0:T(8,128)(2,1)}) fusion(f32[2048]{0:T(1024)S(1)} %copy-done.3, f32[1024]{0:T(1024)S(1)} %add_rsqrt_fusion.2, f32[2048]{0:T(1024)S(1)} %bitcast.26, bf16[1024,2048]{1,0:T(8,128)(2,1)} %all-reduce.3.cloned.1.call-done, bf16[1024,2048]{1,0:T(8,128)(2,1)S(1)} %copy-done), kind=kLoop, calls=%fused_computation.5 | loop fusion | flops 20970496 | bytes 12607488 | tf_op jit(solution)/shard_map/reduce_sum | solution.py:91
  224.4 118.5 %all-gather.17.cloned.1.call-done = bf16[2048,2048]{1,0:T(8,128)(2,1)} async-done(((bf16[256,2048]{1,0:T(8,128)(2,1)}), bf16[2048,2048]{1,0:T(8,128)(2,1)}) %all-gather.17.cloned.1.call-update) | async-done | bytes 8388624 | tf_op jit(solution)/shard_map/all_gather | solution.py:95
  342.9 125.2 %all-gather.19.cloned.1.call-done = bf16[2048,2048]{1,0:T(8,128)(2,1)} async-done(((bf16[2048,256]{1,0:T(8,128)(2,1)}), bf16[2048,2048]{1,0:T(8,128)(2,1)}) %all-gather.19.cloned.1.call-update) | async-done | bytes 8388624 | tf_op jit(solution)/shard_map/all_gather | solution.py:98
  468.1 25.6 %fusion.16 = bf16[1024,2048]{1,0:T(8,128)(2,1)} fusion(bf16[2048,2048]{1,0:T(8,128)(2,1)} %all-gather.19.cloned.1.call-done, bf16[2048,2048]{1,0:T(8,128)(2,1)} %all-gather.17.cloned.1.call-done, bf16[1024,2048]{1,0:T(8,128)(2,1)} %get-tuple-element.10, f32[2048]{0:T(1024)S(1)} %copy-done.10, f32[2048]{0:T(1024)S(1)} %copy-done.11, ...), kind=kOutput, calls=%fused_computation.24 | convolution fusion | flops 17198743552 | bytes 25186304 | tf_op jit(solution)/shard_map/dot_general | solution.py:99
  494.5 17.7 %all-gather.1 = f32[8,1,256]{2,1,0:T(1,128)S(1)} all-gather(f32[1,1,256]{2,1,0:T(1,128)S(1)} %bitcast.36), channel_id=1, replica_groups=mesh['rep'=2,'fs'=8,'tp'=2] {'fs'}, dimensions={0}, use_global_device_ids=true | all-gather | bytes 9216 | tf_op jit(solution)/shard_map/all_gather | solution.py:38
  512.2 2.2 multiply_reduce_fusion.1
  514.4 2.5 psum.31
  516.9 4.5 add_convert_fusion
  (57 shorter events, 9.2 us)
Async XLA Ops:
  6.5 4.5 copy-start.2
  6.5 18.8 %all-gather.9.cloned.1.call-start = ((), (), s32[]{:S(2)}) async-start(), calls=%async_computation.1 | async-start | bytes 6291456 | tf_op jit(solution)/shard_map/all_gather | solution.py:35
  7.3 70.5 %copy-start.9 = (f32[2048]{0:T(1024)S(1)}, f32[2048]{0:T(1024)}, u32[]{:S(2)}) copy-start(f32[2048]{0:T(1024)} %param.19) | copy-start | bytes 24580
  7.3 70.5 %copy-start.12 = (f32[512]{0:T(512)S(1)}, f32[512]{0:T(512)}, u32[]{:S(2)}) copy-start(f32[512]{0:T(512)} %param.23) | copy-start | bytes 6148
  7.3 70.4 %all-gather.13.cloned.1.call-start = ((), (), s32[]{:S(2)}) async-start(), calls=%async_computation.3 | async-start | bytes 2359296 | tf_op jit(solution)/shard_map/all_gather | solution.py:52
  9.1 118.4 %all-gather.11.cloned.1.call-start = ((), (), s32[]{:S(2)}) async-start(), calls=%async_computation.2 | async-start | bytes 2359296 | tf_op jit(solution)/shard_map/all_gather | solution.py:47
  11.0 167.3 %all-gather.15.cloned.1.call-start = ((), (), s32[]{:S(2)}) async-start(), calls=%async_computation.4 | async-start | bytes 2359296 | tf_op jit(solution)/shard_map/all_gather | solution.py:79
  11.8 203.5 %all-reduce.3.cloned.1.call-start = ((), (), s32[]{:S(2)}) async-start(), calls=%async_computation.5 | async-start | bytes 8388608 | tf_op jit(solution)/shard_map/psum | solution.py:82
  28.4 57.7 %copy-start.6 = (f32[512]{0:T(512)S(1)}, f32[512]{0:T(512)}, u32[]{:S(2)}) copy-start(f32[512]{0:T(512)} %param.24) | copy-start | bytes 6148
  83.5 5.0 copy-start.4
  93.6 84.7 %copy-start.13 = (f32[512]{0:T(512)S(1)}, f32[512]{0:T(512)}, u32[]{:S(2)}) copy-start(f32[512]{0:T(512)} %param.22) | copy-start | bytes 6148
  188.7 1.6 copy-start.1
  188.7 5.8 %copy-start.7 = (f32[256]{0:T(256)S(1)}, f32[256]{0:T(256)}, u32[]{:S(2)}) copy-start(f32[256]{0:T(256)} %param.28) | copy-start | bytes 3076
  188.7 154.2 %all-gather.17.cloned.1.call-start = ((), (), s32[]{:S(2)}) async-start(), calls=%async_computation.6 | async-start | bytes 9437184 | tf_op jit(solution)/shard_map/all_gather | solution.py:95
  191.5 27.3 %copy-start.3 = (f32[2048]{0:T(1024)S(1)}, f32[2048]{0:T(1024)}, u32[]{:S(2)}) copy-start(f32[2048]{0:T(1024)} %param.29) | copy-start | bytes 24580
  191.5 276.6 %all-gather.19.cloned.1.call-start = ((), (), s32[]{:S(2)}) async-start(), calls=%async_computation.7 | async-start | bytes 9437184 | tf_op jit(solution)/shard_map/all_gather | solution.py:98
  194.5 317.7 %reduce-scatter.2.cloned.1.call-start = ((), (), s32[]{:S(2)}) async-start(), calls=%async_computation.8 | async-start | bytes 6291456 | tf_op jit(solution)/shard_map/reduce_scatter | solution.py:102
  215.3 3.5 copy-start
  218.8 249.3 %copy-start.10 = (f32[2048]{0:T(1024)S(1)}, f32[2048]{0:T(1024)}, u32[]{:S(2)}) copy-start(f32[2048]{0:T(1024)} %param.32) | copy-start | bytes 24580
  218.8 249.3 %copy-start.11 = (f32[2048]{0:T(1024)S(1)}, f32[2048]{0:T(1024)}, u32[]{:S(2)}) copy-start(f32[2048]{0:T(1024)} %param.30) | copy-start | bytes 24580
  493.8 0.7 copy-start.8
  493.8 18.4 %copy-start.5 = (f32[2048]{0:T(1024)S(1)}, f32[2048]{0:T(1024)}, u32[]{:S(2)}) copy-start(f32[2048]{0:T(1024)} %param.35) | copy-start | bytes 24580
Sparse Core Ops, SparseCore 0:
  8.9 16.3 all-gather.8
  27.4 50.2 all-gather.12
  79.8 47.6 all-gather.10
  129.4 48.8 all-gather.14
  188.8 26.3 all-reduce.2
  217.3 125.6 all-gather.16
  345.0 123.1 all-gather.18
  493.9 10.0 reduce-scatter.1
where the time goes:
time: 529 us; the launch traced here: 528 us
  waiting for transfers between devices  392 us (74%)
  matrix products  44.2 us (8%)
  blocking collectives  40.4 us (8%)
  other arithmetic  27.6 us (5%)
  between operations  13.7 us (3%)
  local copies, waits for them, and re-layouts  10.5 us (2%)
    all_gather x1, waiting for transfers between devices, local(): whole_down = lax.all_gather(down_half, 'fs', axis=1, tiled=True)  125 us
    all_gather x1, waiting for transfers between devices, local(): whole_up = lax.all_gather(up_half, 'fs', axis=0, tiled=True)  119 us
    all_gather x1, waiting for transfers between devices, local(): lax.all_gather(out_weight.astype(jnp.bfloat16), 'fs', axis=1, tiled=True)  50.8 us
    all_gather x1, waiting for transfers between devices, local(): lax.all_gather(v_weight.astype(jnp.bfloat16), 'fs', axis=0, tiled=True)  49.3 us
    all_gather x1, waiting for transfers between devices, local(): lax.all_gather(u_weight.astype(jnp.bfloat16), 'fs', axis=0, tiled=True)  30.4 us
    dot_general x1, matrix products, local(): terms = jnp.dot(hidden, whole_down, preferred_element_type=jnp.float32)  25.6 us
    all_gather x1, blocking collectives, local(): lax.all_gather(down_scale, 'fs', axis=0, tiled=True)  17.7 us
    all_gather x1, blocking collectives, local(): lax.all_gather(out_scale, 'fs', axis=0, tiled=True)  17.7 us
  transfers between devices with their start and end apart: 8, of which 7 were waited for; matrix products, arithmetic and copies ran while one was open for 7% of the time, Pallas kernels for 0%

commit v1 on v0

--- a/solution.py
+++ b/solution.py
@@ -1,7 +1,124 @@
+import functools
+
 import jax
 import jax.numpy as jnp
 from jax import lax
+from jax.experimental import pallas as pl
+from jax.experimental.pallas import tpu as pltpu
 from jax.sharding import PartitionSpec as P
+
+
+def gather_kernel(by_rows, n_out, n_in, *refs):
+    count = len(by_rows)
+    srcs, resid = refs[:count], refs[count]
+    dsts, other = refs[count + 1 : 2 * count + 1], refs[2 * count + 1]
+    z_send, z_recv, y_send, y_recv, x_send, x_recv, t_send, t_recv, own_sem = refs[2 * count + 2 :]
+    member = lax.axis_index("fs")
+    rep = lax.axis_index("rep")
+    tp = lax.axis_index("tp")
+    outer, inner = member // n_in, member % n_in
+    peer_in = 1 - inner
+
+    def at(index):
+        return {"fs": index}
+
+    barrier = pltpu.get_barrier_semaphore()
+    greeted = [at(lax.rem(outer + k, n_out) * n_in + inner) for k in range(1, n_out)]
+    greeted += [at(outer * n_in + peer_in), {"rep": 1 - rep}, {"tp": 1 - tp}]
+    for device in greeted:
+        pl.semaphore_signal(barrier, inc=1, device_id=device, device_id_type=pl.DeviceIdType.MESH)
+    pl.semaphore_wait(barrier, len(greeted))
+
+    def slot(w, index, half=None):
+        rows, cols = srcs[w].shape
+        base, size = (0, rows) if half is None else (half * (rows // 2), rows // 2)
+        if by_rows[w]:
+            return dsts[w].at[pl.ds(pl.multiple_of(index * rows + base, 8), size), :]
+        return dsts[w].at[pl.ds(base, size), pl.ds(pl.multiple_of(index * cols, 128), cols)]
+
+    def remote(src, dst, send, recv, device):
+        return pltpu.make_async_remote_copy(
+            src_ref=src,
+            dst_ref=dst,
+            send_sem=send,
+            recv_sem=recv,
+            device_id=device,
+            device_id_type=pl.DeviceIdType.MESH,
+        )
+
+    swap = remote(resid, other, t_send, t_recv, {"tp": 1 - tp})
+    swap.start()
+    own, z_copies, y_copies, x_copies = [], {}, {}, {}
+    for w in range(count):
+        for k in range(1, n_out):
+            target = lax.rem(outer - k + n_out, n_out) * n_in + inner
+            copy = remote(srcs[w], slot(w, member), z_send.at[w, k - 1], z_recv.at[w, k - 1], at(target))
+            copy.start()
+            z_copies[w, k] = copy
+        local_copy = pltpu.make_async_copy(srcs[w], slot(w, member), own_sem.at[w])
+        local_copy.start()
+        own.append(local_copy)
+
+    def cross_inner(w, k):
+        index = lax.rem(outer + k, n_out) * n_in + inner
+        rows = srcs[w].shape[0]
+        if k:
+            z_copies[w, k].wait_recv()
+            source = slot(w, index, rep)
+        else:
+            source = srcs[w].at[pl.ds(pl.multiple_of(rep * (rows // 2), 8), rows // 2), :]
+        copy = remote(source, slot(w, index, rep), y_send.at[w, k], y_recv.at[w, k], at(outer * n_in + peer_in))
+        copy.start()
+        y_copies[w, k] = copy
+
+    def cross_rep(w, k):
+        index = lax.rem(outer + k, n_out) * n_in + peer_in
+        y_copies[w, k].wait_recv()
+        landed = slot(w, index, rep)
+        copy = remote(landed, landed, x_send.at[w, k], x_recv.at[w, k], {"rep": 1 - rep})
+        copy.start()
+        x_copies[w, k] = copy
+
+    order = [(w, k) for w in range(count) for k in range(n_out)]
+    lag = 2
+    for step in range(len(order) + lag):
+        if step < len(order):
+            cross_inner(*order[step])
+        if step >= lag:
+            cross_rep(*order[step - lag])
+    for item in order:
+        x_copies[item].wait()
+        y_copies[item].wait_send()
+    for copy in z_copies.values():
+        copy.wait_send()
+    for copy in own:
+        copy.wait()
+    swap.wait()
+
+
+def gather_all(shards, by_rows, resid):
+    members = lax.axis_size("fs")
+    n_in = 2
+    n_out = members // n_in
+    count = len(shards)
+    shapes = []
+    for shard, rowwise in zip(shards, by_rows):
+        rows, cols = shard.shape
+        full = (rows * members, cols) if rowwise else (rows, cols * members)
+        shapes.append(jax.ShapeDtypeStruct(full, shard.dtype))
+    shapes.append(jax.ShapeDtypeStruct(resid.shape, resid.dtype))
+    pairs = [(count, n_out - 1)] * 2 + [(count, n_out)] * 4
+    return pl.pallas_call(
+        functools.partial(gather_kernel, by_rows, n_out, n_in),
+        out_shape=shapes,
+        in_specs=[pl.BlockSpec(memory_space=pltpu.VMEM)] * (count + 1),
+        out_specs=[pl.BlockSpec(memory_space=pl.ANY)] * (count + 1),
+        scratch_shapes=[pltpu.SemaphoreType.DMA(pair) for pair in pairs]
+        + [pltpu.SemaphoreType.DMA, pltpu.SemaphoreType.DMA, pltpu.SemaphoreType.DMA((count,))],
+        compiler_params=pltpu.CompilerParams(
+            collective_id=0, has_side_effects=True, vmem_limit_bytes=32 * 1024 * 1024
+        ),
+    )(*shards, resid)
 
 
 def rms_norm(values, gain, width, power_sum):
@@ -111,6 +228,127 @@
     )
 
 
+def local_fast(
+    resid,
+    gain_mix_in,
+    u_weight,
+    v_weight,
+    u_scale,
+    v_scale,
+    v_gain,
+    mix_matrix,
+    mix_bias,
+    out_weight,
+    out_scale,
+    gain_mix_out,
+    gain_ffn_in,
+    up_weight,
+    up_scale,
+    down_weight,
+    down_scale,
+    gain_ffn_out,
+):
+    rows = resid.shape[0]
+    part_width = resid.shape[1]
+    width = part_width * lax.axis_size("tp")
+    lane = lax.axis_index("tp")
+    half = jnp.bfloat16
+    scale_cols = out_scale.shape[0]
+    scales = jnp.concatenate(
+        [jnp.broadcast_to(out_scale, (8, scale_cols)), jnp.broadcast_to(down_scale, (8, scale_cols))]
+    )
+    shards = [
+        v_weight.astype(half),
+        u_weight.astype(half),
+        out_weight.astype(half),
+        scales,
+        up_weight.astype(half),
+        down_weight.astype(half),
+    ]
+    whole_v, whole_u, whole_out, whole_scales, whole_up, whole_down, other = gather_all(
+        shards, (True, True, False, True, True, False), resid
+    )
+    whole_scales = whole_scales.reshape(-1, 16, scale_cols)
+    out_scales, down_scales = whole_scales[:, 0].reshape(-1), whole_scales[:, 8].reshape(-1)
+    swap = [(0, 1), (1, 0)]
+    full_rows = jnp.where(
+        lane == 0,
+        jnp.concatenate([resid, other], axis=1),
+        jnp.concatenate([other, resid], axis=1),
+    )
+    full_float = full_rows.astype(jnp.float32)
+    normed = rms_norm(
+        full_float, gain_mix_in, width, jnp.sum(full_float * full_float, axis=1, keepdims=True)
+    ).astype(jnp.bfloat16)
+    branch_cols = u_weight.shape[1]
+    u_pre = jnp.dot(
+        normed,
+        whole_u,
+        preferred_element_type=jnp.float32,
+    )
+    v_pre = jnp.dot(
+        normed,
+        whole_v,
+        preferred_element_type=jnp.float32,
+    )
+    u_act = jax.nn.gelu(u_pre * u_scale)
+    v_act = jax.nn.gelu(v_pre * v_scale)
+    total, squares = lax.psum(
+        (jnp.sum(v_act, axis=1, keepdims=True), jnp.sum(v_act * v_act, axis=1, keepdims=True)), "tp"
+    )
+    branch_width = branch_cols * lax.axis_size("tp")
+    centre = total / branch_width
+    spread = squares / branch_width - centre * centre
+    v_norm = ((v_act - centre) * lax.rsqrt(spread + 1e-06) * v_gain).astype(jnp.bfloat16)
+    groups = mix_matrix.shape[0]
+    block = mix_matrix.shape[1]
+    blocks = v_norm.reshape(rows // block, block, groups, branch_cols // groups)
+    mixed = (
+        jnp.einsum(
+            "gts,bsgd->btgd",
+            mix_matrix.astype(jnp.bfloat16),
+            blocks,
+            preferred_element_type=jnp.float32,
+        )
+        + mix_bias.T[None, :, :, None]
+    )
+    gated = (u_act * mixed.reshape(rows, branch_cols)).astype(jnp.bfloat16)
+    partial_value = jnp.dot(
+        gated,
+        whole_out,
+        preferred_element_type=jnp.float32,
+    )
+    rounded = partial_value.astype(half)
+    mix_out = (
+        rounded.astype(jnp.float32) + lax.ppermute(rounded, "tp", swap).astype(jnp.float32)
+    ) * out_scales
+    power = jnp.sum(mix_out * mix_out, axis=1, keepdims=True)
+    middle_full = (full_float + rms_norm(mix_out, gain_mix_out, width, power)).astype(jnp.bfloat16)
+    middle = lax.dynamic_slice_in_dim(middle_full, lane * part_width, part_width, 1)
+    middle_float = middle_full.astype(jnp.float32)
+    ffn_in = rms_norm(
+        middle_float,
+        gain_ffn_in,
+        width,
+        jnp.sum(middle_float * middle_float, axis=1, keepdims=True),
+    ).astype(jnp.bfloat16)
+    raised = jnp.dot(ffn_in, whole_up, preferred_element_type=jnp.float32)
+    hidden = jnp.square(jax.nn.relu(raised * up_scale)).astype(jnp.bfloat16)
+    terms = jnp.dot(hidden, whole_down, preferred_element_type=jnp.float32)
+    own_down = lax.dynamic_slice_in_dim(down_scales, lane * part_width, part_width, 0)
+    terms = terms.astype(half)
+    kept = lax.dynamic_slice_in_dim(terms, lane * part_width, part_width, 1)
+    sent = lax.dynamic_slice_in_dim(terms, (1 - lane) * part_width, part_width, 1)
+    ffn_out = (
+        kept.astype(jnp.float32) + lax.ppermute(sent, "tp", swap).astype(jnp.float32)
+    ) * own_down
+    power_out = lax.psum(jnp.sum(ffn_out * ffn_out, axis=1, keepdims=True), "tp")
+    own_gain_out = lax.dynamic_slice_in_dim(gain_ffn_out, lane * part_width, part_width, 0)
+    return (middle.astype(jnp.float32) + rms_norm(ffn_out, own_gain_out, width, power_out)).astype(
+        jnp.bfloat16
+    )
+
+
 def solution(mesh):
     in_specs = (
         P(("rep", "fs"), "tp"),
@@ -133,4 +371,18 @@
         P(),
     )
     out_specs = P(("rep", "fs"), "tp")
-    return jax.shard_map(local, mesh=mesh, in_specs=in_specs, out_specs=out_specs, check_vma=False)
+    sizes = mesh.shape
+
+    def whole(*args):
+        columns = args[9].shape[1] // sizes["fs"]
+        depth = args[2].shape[0] // sizes["fs"]
+        paired = sizes["rep"] == 2 and sizes["tp"] == 2 and sizes["fs"] % 2 == 0
+        fast = paired and columns % 128 == 0 and depth % 32 == 0
+        return mapped(local_fast if fast else local)(*args)
+
+    def mapped(body):
+        return jax.shard_map(
+            body, mesh=mesh, in_specs=in_specs, out_specs=out_specs, check_vma=False
+        )
+
+    return whole

time: 529 us -> 414 us (0.78)
  waiting for transfers between devices: 392 us -> 11.5 us
  Pallas kernels: 0 us -> 303 us
  blocking collectives: 40.4 us -> 4.97 us
  between operations: 13.7 us -> 0.25 us
  local copies, waits for them, and re-layouts: 10.5 us -> 17 us
    all_gather x6 -> x0, waiting for transfers between devices: 388 us -> none  [the longest x1 125 us: local(): whole_down = lax.all_gather(down_half, 'fs', axis=1, tiled=True)]
    pallas_call x0 -> x1, Pallas kernels: none -> 303 us  [gather_all(): pl.pallas_call(functools.partial(gather_kernel, by_rows, n_out, n_in), ou...]
    all_gather x2 -> x0, blocking collectives: 35.4 us -> none  [the longest x1 17.7 us: local(): lax.all_gather(down_scale, 'fs', axis=0, tiled=True)]
    ppermute x0 -> x2, waiting for transfers between devices: none -> 11.5 us  [the longest x1 7.32 us: local_fast(): lax.ppermute(rounded, 'tp', swap).astype(jnp.float32)]
  transfers between devices with their start and end apart: 8 -> 2, of which waited for: 7 -> 2; matrix products, arithmetic and copies ran while one was open for 7% -> 0% of each run, Pallas kernels for 0% -> 0%
where the time goes in v1:
time: 414 us; the launch traced here: 413 us
  Pallas kernels  303 us (73%)
  matrix products  45 us (11%)
  other arithmetic  31.2 us (8%)
  local copies, waits for them, and re-layouts  17 us (4%)
  waiting for transfers between devices  11.5 us (3%)
  blocking collectives  4.97 us (1%)
    pallas_call x1, Pallas kernels, gather_all(): pl.pallas_call(functools.partial(gather_kernel, by_rows, n_out, n_in), ou...  303 us
    dot_general x1, matrix products, local_fast(): terms = jnp.dot(hidden, whole_down, preferred_element_type=jnp.float32)  25.9 us
    dot_general x1, matrix products, local_fast(): jnp.dot(gated, whole_out, preferred_element_type=jnp.float32)  10.1 us
    reshape x2, local copies, waits for them, and re-layouts, local_fast(): gated = (u_act * mixed.reshape(rows, branch_cols)).astype(jnp.bfloat16)  8.6 us
  transfers between devices with their start and end apart: 2, of which 2 were waited for; matrix products, arithmetic and copies ran while one was open for 0% of the time, Pallas kernels for 0%

profile of v1, /device:TPU:0, one launch (start us, length us, event | category | flops | bytes accessed | tf_op | source)
XLA Modules:
  0.0 413.1 jit_solution(7822514284807597804)
XLA Ops:
  0.0 1.2 convert_element_type.67.refs_1_
  1.2 2.0 convert_element_type.66.refs_0_
  3.2 1.8 convert_element_type.68.refs_2_
  5.0 1.7 convert_element_type.69.refs_4_
  7.9 1.2 copy-done.3
  11.0 302.8 %shard_map.172 = (bf16[2048,512]{1,0:T(8,128)(2,1)S(1)}, bf16[2048,512]{1,0:T(8,128)(2,1)S(1)}, bf16[512,2048]{1,0:T(8,128)(2,1)S(1)}, f32[128,256]{1,0:T(8,128)...) custom-call(bf16[256,512]{1,0:T(8,128)(2,1)S(1)} %copy-done.4, ...), custom_call_target="tpu_custom_call" | custom-call | tf_op jit(solution)/shard_map/pallas_call | solution.py:111
  313.8 1.5 fusion.3
  315.4 5.3 %fusion.50 = (f32[1024]{0:T(1024)S(1)}, f32[1024]{0:T(1024)S(1)}, f32[1024,512]{1,0:T(8,128)}) fusion(f32[512]{0:T(512)S(1)} %copy-done.19, bf16[2048,512]{1,0:T(8,128)(2,1)S(1)} %get-tuple-element.14, f32[2048]{0:T(1024)S(1)} %copy-done.16, f32[1024]{0:T(1024)S(1)} %add_rsqrt_fusion.4, bf16[1024,1024]{1,0:T(8,128)(2,1)S(1)} %copy-done, ...), kind=kOutput, calls=%fused_computation.64 | convolution fusion | flops 2181036032 | bytes 8411137 | tf_op jit(solution)/shard_map/dot_general | solution.py:289
  320.7 2.5 all-reduce
  323.2 1.9 multiply_convert_fusion.1
  325.2 2.1 reshape.48
  327.3 3.8 bitcast_add_fusion
  331.1 3.8 copy.31
  334.9 4.8 %reshape.49 = f32[1024,512]{1,0:T(8,128)} reshape(f32[8,128,8,64]{3,2,1,0:T(8,128)} %copy.31) | data formatting | bytes 4194304 | tf_op jit(solution)/shard_map/reshape | solution.py:315
  339.7 10.1 %convolution_convert_fusion = bf16[1024,2048]{1,0:T(8,128)(2,1)} fusion(bf16[512,2048]{1,0:T(8,128)(2,1)} %copy-done.8, f32[1024,512]{1,0:T(8,128)} %reshape.49, bf16[2048,512]{1,0:T(8,128)(2,1)} %copy-done.7, f32[2048]{0:T(1024)S(1)} %copy-done.16, f32[1024]{0:T(1024)S(1)} %add_rsqrt_fusion.4, f32[512]{0:T(512)S(1)} %copy-done.20, ...), kind=kOutput, calls=%fused_computation.24 | convolution fusion | flops 4330094592 | bytes 14694401 | tf_op jit(solution)/shard_map/dot_general | solution.py:316
  349.9 7.3 %collective-permute-done = bf16[1024,2048]{1,0:T(8,128)(2,1)} collective-permute-done((bf16[1024,2048]{1,0:T(8,128)(2,1)}, bf16[1024,2048]{1,0:T(8,128)(2,1)}, u32[]{:S(2)}, u32[]{:S(2)}) %collective-permute-start) | collective-permute-done | bytes 4194336 | tf_op jit(solution)/shard_map/ppermute | solution.py:323
  357.3 5.3 %multiply_reduce_fusion = f32[1024]{0:T(1024)S(1)} fusion(bf16[1024,2048]{1,0:T(8,128)(2,1)} %collective-permute-done, bf16[1024,2048]{1,0:T(8,128)(2,1)} %convolution_convert_fusion, f32[2048]{0:T(1024)S(1)} %bitcast.25), kind=kLoop, calls=%fused_computation.13 | loop fusion | flops 12581888 | bytes 8400896 | tf_op jit(solution)/shard_map/reduce_sum | solution.py:325
  362.6 7.4 %fusion = (f32[1024]{0:T(1024)S(1)}, bf16[1024,2048]{1,0:T(8,128)(2,1)}) fusion(f32[2048]{0:T(1024)S(1)} %copy-done.11, f32[1024]{0:T(1024)S(1)} %add_rsqrt_fusion.2, f32[2048]{0:T(1024)S(1)} %bitcast.26, bf16[1024,2048]{1,0:T(8,128)(2,1)} %collective-permute-done, bf16[1024,2048]{1,0:T(8,128)(2,1)S(1)} %copy-done.9, bf16[1024,1024]{1,0:T(8,128)(2,1)S(1)} %copy-done, ...), kind=kLoop, calls=%fused_computation.5 | loop fusion | flops 44039168 | bytes 16801792 | tf_op jit(solution)/shard_map/reduce_sum | solution.py:333
  370.0 25.9 %fusion.16 = bf16[1024,2048]{1,0:T(8,128)(2,1)} fusion(bf16[2048,2048]{1,0:T(8,128)(2,1)} %get-tuple-element.18, bf16[2048,2048]{1,0:T(8,128)(2,1)} %copy-done.6, bf16[1024,2048]{1,0:T(8,128)(2,1)} %get-tuple-element.24, f32[2048]{0:T(1024)S(1)} %copy-done.17, f32[2048]{0:T(1024)S(1)} %copy-done.18, f32[1024]{0:T(1024)S(1)} %add_rsqrt_fusion.1), kind=kOutput, calls=%fused_computation.25 | convolution fusion | flops 17198743552 | bytes 25186304 | tf_op jit(solution)/shard_map/dot_general | solution.py:337
  395.9 3.1 constant_dynamic-slice_fusion
  399.2 4.2 %collective-permute-done.1 = bf16[1024,1024]{1,0:T(8,128)(2,1)S(1)} collective-permute-done((bf16[1024,1024]{1,0:T(8,128)(2,1)}, bf16[1024,1024]{1,0:T(8,128)(2,1)S(1)}, u32[]{:S(2)}, u32[]{:S(2)}) %collective-permute-start.1) | collective-permute-done | bytes 2097184 | tf_op jit(solution)/shard_map/ppermute | solution.py:343
  403.4 2.5 multiply_reduce_fusion.1
  405.8 2.5 psum.23
  408.3 4.7 %add_convert_fusion = bf16[1024,1024]{1,0:T(8,128)(2,1)} fusion(bf16[1024,1024]{1,0:T(8,128)(2,1)S(1)} %collective-permute-done.1, f32[1024]{0:T(1024)S(1)} %dynamic-slice-done, f32[1024]{0:T(1024)S(1)} %bitcast.28, f32[1024]{0:T(1024)S(1)} %dynamic_slice.18, bf16[1024,2048]{1,0:T(8,128)(2,1)} %get-tuple-element.24, s32[]{:T(128)} %select_n.19, ...), kind=kLoop, calls=%fused_computation.17 | loop fusion | flops 9437184 | bytes 8400900 | tf_op jit(solution)/shard_map/convert_element_type | solution.py:347
  (56 shorter events, 3.5 us)
Async XLA Ops:
  0.0 6.7 %copy-start.10 = (f32[2048,256]{1,0:T(8,128)S(1)}, f32[2048,256]{1,0:T(8,128)}, u32[]{:S(2)}) copy-start(f32[2048,256]{1,0:T(8,128)} %param.33) | copy-start | bytes 6291460
  0.0 7.8 %copy-start.14 = (f32[256]{0:T(256)S(1)}, f32[256]{0:T(256)}, u32[]{:S(2)}) copy-start(f32[256]{0:T(256)} %param.28) | copy-start | bytes 3076
  0.0 7.8 %copy-start.15 = (f32[256]{0:T(256)S(1)}, f32[256]{0:T(256)}, u32[]{:S(2)}) copy-start(f32[256]{0:T(256)} %param.34) | copy-start | bytes 3076
  0.0 7.8 %copy-start = (bf16[1024,1024]{1,0:T(8,128)(2,1)S(1)}, bf16[1024,1024]{1,0:T(8,128)(2,1)}, u32[]{:S(2)}) copy-start(bf16[1024,1024]{1,0:T(8,128)(2,1)} %refs_6_.1) | copy-start | bytes 6291460
  7.8 1.2 copy-start.3
  9.1 0.9 copy-start.4
  10.0 0.9 copy-start.5
  11.0 304.4 %copy-start.16 = (f32[2048]{0:T(1024)S(1)}, f32[2048]{0:T(1024)}, u32[]{:S(2)}) copy-start(f32[2048]{0:T(1024)} %param.19) | copy-start | bytes 24580
  11.0 304.4 %copy-start.19 = (f32[512]{0:T(512)S(1)}, f32[512]{0:T(512)}, u32[]{:S(2)}) copy-start(f32[512]{0:T(512)} %param.23) | copy-start | bytes 6148
  313.8 6.9 %copy-start.1 = (bf16[1024,1024]{1,0:T(8,128)(2,1)}, bf16[1024,1024]{1,0:T(8,128)(2,1)S(1)}, u32[]{:S(2)}) copy-start(bf16[1024,1024]{1,0:T(8,128)(2,1)S(1)} %get-tuple-element.12) | copy-start | bytes 6291460
  313.8 6.9 %copy-start.6 = (bf16[2048,2048]{1,0:T(8,128)(2,1)}, bf16[2048,2048]{1,0:T(8,128)(2,1)S(1)}, u32[]{:S(2)}) copy-start(bf16[2048,2048]{1,0:T(8,128)(2,1)S(1)} %get-tuple-element.17) | copy-start | bytes 25165828
  313.8 6.9 %copy-start.7 = (bf16[2048,512]{1,0:T(8,128)(2,1)}, bf16[2048,512]{1,0:T(8,128)(2,1)S(1)}, u32[]{:S(2)}) copy-start(bf16[2048,512]{1,0:T(8,128)(2,1)S(1)} %get-tuple-element.13) | copy-start | bytes 6291460
  313.8 6.9 %copy-start.8 = (bf16[512,2048]{1,0:T(8,128)(2,1)}, bf16[512,2048]{1,0:T(8,128)(2,1)S(1)}, u32[]{:S(2)}) copy-start(bf16[512,2048]{1,0:T(8,128)(2,1)S(1)} %get-tuple-element.15) | copy-start | bytes 6291460
  315.4 7.9 %copy-start.13 = (f32[512]{0:T(512)S(1)}, f32[512]{0:T(512)}, u32[]{:S(2)}) copy-start(f32[512]{0:T(512)} %param.24) | copy-start | bytes 6148
  320.7 6.6 %copy-start.12 = (f32[8,128]{1,0:T(8,128)S(1)}, f32[8,128]{1,0:T(8,128)}, u32[]{:S(2)}) copy-start(f32[8,128]{1,0:T(8,128)} %param.26) | copy-start | bytes 12292
  334.8 4.8 %copy-start.20 = (f32[512]{0:T(512)S(1)}, f32[512]{0:T(512)}, u32[]{:S(2)}) copy-start(f32[512]{0:T(512)} %param.22) | copy-start | bytes 6148
  349.8 7.5 %collective-permute-start = (bf16[1024,2048]{1,0:T(8,128)(2,1)}, bf16[1024,2048]{1,0:T(8,128)(2,1)}, u32[]{:S(2)}, u32[]{:S(2)}) collective-permute-start(bf16[1024,2048]{1,0:T(8,128)(2,1)} %convolution_convert_fusion), channel_id=1, source_target_pairs={{0,1},{1,0},{2,3},{3,2},{4,5},{5,4},{6,7},{7,6},{8,9},{9,8},{10,11... | collective-permute-start | bytes 12582920 | tf_op jit(solution)/shard_map/ppermute | solution.py:323
  357.3 5.3 %copy-start.2 = (bf16[1024,1024]{1,0:T(8,128)(2,1)S(1)}, bf16[1024,1024]{1,0:T(8,128)(2,1)}, u32[]{:S(2)}) copy-start(bf16[1024,1024]{1,0:T(8,128)(2,1)} %copy-done.1) | copy-start | bytes 6291460
  357.3 5.3 %copy-start.9 = (bf16[1024,2048]{1,0:T(8,128)(2,1)S(1)}, bf16[1024,2048]{1,0:T(8,128)(2,1)}, u32[]{:S(2)}) copy-start(bf16[1024,2048]{1,0:T(8,128)(2,1)} %convolution_convert_fusion) | copy-start | bytes 12582916
  357.3 5.3 %copy-start.11 = (f32[2048]{0:T(1024)S(1)}, f32[2048]{0:T(1024)}, u32[]{:S(2)}) copy-start(f32[2048]{0:T(1024)} %param.29) | copy-start | bytes 24580
  362.6 7.4 %copy-start.17 = (f32[2048]{0:T(1024)S(1)}, f32[2048]{0:T(1024)}, u32[]{:S(2)}) copy-start(f32[2048]{0:T(1024)} %param.32) | copy-start | bytes 24580
  362.6 7.4 %copy-start.18 = (f32[2048]{0:T(1024)S(1)}, f32[2048]{0:T(1024)}, u32[]{:S(2)}) copy-start(f32[2048]{0:T(1024)} %param.30) | copy-start | bytes 24580
  399.0 4.4 %collective-permute-start.1 = (bf16[1024,1024]{1,0:T(8,128)(2,1)}, bf16[1024,1024]{1,0:T(8,128)(2,1)S(1)}, u32[]{:S(2)}, u32[]{:S(2)}) collective-permute-start(bf16[1024,1024]{1,0:T(8,128)(2,1)} %constant_dynamic-slice_fusion), channel_id=1, source_target_pairs={{0,1},{1,0},{2,3},{3,2},{4,5},{5,4},{6,7},{7,6},{8,9},{9,8},{10,11... | collective-permute-start | bytes 6291464 | tf_op jit(solution)/shard_map/ppermute | solution.py:343
  399.2 9.2 %dynamic-slice-start = ((f32[2048]{0:T(1024)}, s32[]{:T(128)}), f32[1024]{0:T(1024)S(1)}, s32[]{:S(2)}) async-start(f32[2048]{0:T(1024)} %param.35, s32[]{:T(128)} %select_n.19), calls=%async_computation | async-start | bytes 8704 | tf_op jit(solution)/shard_map/dynamic_slice | solution.py:346

commit v2 on v1

--- a/solution.py
+++ b/solution.py
@@ -8,7 +8,7 @@
 from jax.sharding import PartitionSpec as P
 
 
-def gather_kernel(by_rows, n_out, n_in, *refs):
+def gather_kernel(by_rows, parts, n_out, n_in, *refs):
     count = len(by_rows)
     srcs, resid = refs[:count], refs[count]
     dsts, other = refs[count + 1 : 2 * count + 1], refs[2 * count + 1]
@@ -18,81 +18,166 @@
     tp = lax.axis_index("tp")
     outer, inner = member // n_in, member % n_in
     peer_in = 1 - inner
-
-    def at(index):
-        return {"fs": index}
+    has_left, has_right = outer > 0, outer < n_out - 1
+    left, right = {"fs": member - n_in}, {"fs": member + n_in}
+    across, twin, mate = {"fs": outer * n_in + peer_in}, {"rep": 1 - rep}, {"tp": 1 - tp}
+
+    def greet(device):
+        pl.semaphore_signal(barrier, inc=1, device_id=device, device_id_type=pl.DeviceIdType.MESH)
 
     barrier = pltpu.get_barrier_semaphore()
-    greeted = [at(lax.rem(outer + k, n_out) * n_in + inner) for k in range(1, n_out)]
-    greeted += [at(outer * n_in + peer_in), {"rep": 1 - rep}, {"tp": 1 - tp}]
-    for device in greeted:
-        pl.semaphore_signal(barrier, inc=1, device_id=device, device_id_type=pl.DeviceIdType.MESH)
-    pl.semaphore_wait(barrier, len(greeted))
-
-    def slot(w, index, half=None):
+    for step in (1, n_out - 1):
+        greet({"fs": lax.rem(outer + step, n_out) * n_in + inner})
+    for device in (across, twin, mate):
+        greet(device)
+    pl.semaphore_wait(barrier, 5)
+
+    def slot(part, index, first=0, length=4):
+        w, low, size = parts[part]
         rows, cols = srcs[w].shape
-        base, size = (0, rows) if half is None else (half * (rows // 2), rows // 2)
+        base, size = low + first * (size // 4), length * (size // 4)
         if by_rows[w]:
             return dsts[w].at[pl.ds(pl.multiple_of(index * rows + base, 8), size), :]
-        return dsts[w].at[pl.ds(base, size), pl.ds(pl.multiple_of(index * cols, 128), cols)]
-
-    def remote(src, dst, send, recv, device):
+        return dsts[w].at[
+            pl.ds(pl.multiple_of(base, 8), size), pl.ds(pl.multiple_of(index * cols, 128), cols)
+        ]
+
+    def remote(ref, send, recv, device):
         return pltpu.make_async_remote_copy(
-            src_ref=src,
-            dst_ref=dst,
+            src_ref=ref,
+            dst_ref=ref,
             send_sem=send,
             recv_sem=recv,
             device_id=device,
             device_id_type=pl.DeviceIdType.MESH,
         )
 
-    swap = remote(resid, other, t_send, t_recv, {"tp": 1 - tp})
-    swap.start()
-    own, z_copies, y_copies, x_copies = [], {}, {}, {}
+    swap = pltpu.make_async_remote_copy(
+        src_ref=resid,
+        dst_ref=other,
+        send_sem=t_send,
+        recv_sem=t_recv,
+        device_id=mate,
+        device_id_type=pl.DeviceIdType.MESH,
+    )
+    own = []
     for w in range(count):
-        for k in range(1, n_out):
-            target = lax.rem(outer - k + n_out, n_out) * n_in + inner
-            copy = remote(srcs[w], slot(w, member), z_send.at[w, k - 1], z_recv.at[w, k - 1], at(target))
-            copy.start()
-            z_copies[w, k] = copy
-        local_copy = pltpu.make_async_copy(srcs[w], slot(w, member), own_sem.at[w])
-        local_copy.start()
-        own.append(local_copy)
-
-    def cross_inner(w, k):
-        index = lax.rem(outer + k, n_out) * n_in + inner
-        rows = srcs[w].shape[0]
-        if k:
-            z_copies[w, k].wait_recv()
-            source = slot(w, index, rep)
+        rows, cols = srcs[w].shape
+        if by_rows[w]:
+            place = dsts[w].at[pl.ds(pl.multiple_of(member * rows, 8), rows), :]
         else:
-            source = srcs[w].at[pl.ds(pl.multiple_of(rep * (rows // 2), 8), rows // 2), :]
-        copy = remote(source, slot(w, index, rep), y_send.at[w, k], y_recv.at[w, k], at(outer * n_in + peer_in))
-        copy.start()
-        y_copies[w, k] = copy
-
-    def cross_rep(w, k):
-        index = lax.rem(outer + k, n_out) * n_in + peer_in
-        y_copies[w, k].wait_recv()
-        landed = slot(w, index, rep)
-        copy = remote(landed, landed, x_send.at[w, k], x_recv.at[w, k], {"rep": 1 - rep})
-        copy.start()
-        x_copies[w, k] = copy
-
-    order = [(w, k) for w in range(count) for k in range(n_out)]
-    lag = 2
+            place = dsts[w].at[:, pl.ds(pl.multiple_of(member * cols, 128), cols)]
+        own.append(pltpu.make_async_copy(srcs[w], place, own_sem.at[w]))
+        own[w].start()
+
+    def column(index, line):
+        return index * n_in + line
+
+    def z_copy(part, way, d, piece):
+        ahead = 1 if way == 0 else -1
+        index = column(outer - ahead * d, inner)
+        ref = slot(part, index, 2 * rep, 2) if piece == 0 else slot(part, index, 3 * (1 - rep), 1)
+        return remote(
+            ref,
+            z_send.at[part, way, d, piece],
+            z_recv.at[part, way, d, piece],
+            right if way == 0 else left,
+        )
+
+    def valid(way, d):
+        return outer >= d if way == 0 else outer + d <= n_out - 1
+
+    def onward(way):
+        return has_right if way == 0 else has_left
+
+    def source_of(way, d):
+        return outer - d if way == 0 else outer + d
+
+    def y_copy(part, way, d):
+        ref = slot(part, column(source_of(way, d), inner), 2 * rep, 2)
+        return remote(ref, y_send.at[part, way, d], y_recv.at[part, way, d], across)
+
+    def y_own(part):
+        ref = slot(part, member)
+        return remote(ref, y_send.at[part, 0, 0], y_recv.at[part, 0, 0], across)
+
+    def x_copy(part, way, d, piece):
+        if piece == 0:
+            ref = slot(part, column(source_of(way, d), inner), 1 + rep, 1)
+        else:
+            ref = slot(part, column(source_of(way, d), peer_in), 2 * rep, 2)
+        return remote(ref, x_send.at[part, way, d, piece], x_recv.at[part, way, d, piece], twin)
+
+    def landed(part, way, d, piece):
+        index = column(source_of(way, d), inner)
+        ref = slot(part, index, 2 * rep, 2) if piece == 0 else slot(part, index, 3 * (1 - rep), 1)
+        remote(
+            ref,
+            z_send.at[part, way, d - 1, piece],
+            z_recv.at[part, way, d - 1, piece],
+            left if way == 0 else right,
+        ).wait_recv()
+
+    for w in range(count):
+        own[w].wait()
+        for part, (held, _, _) in enumerate(parts):
+            if held == w:
+                for way in range(2):
+
+                    @pl.when(onward(way))
+                    def _():
+                        z_copy(part, way, 0, 0).start()
+                        z_copy(part, way, 0, 1).start()
+
+                y_own(part).start()
+        if w == 0:
+            swap.start()
+
+    def first_stage(part, way, d):
+        @pl.when(valid(way, d))
+        def _():
+            for piece in range(2):
+                landed(part, way, d, piece)
+                if d < n_out - 1:
+                    pl.when(onward(way))(lambda: z_copy(part, way, d, piece).start())
+                if piece == 0:
+                    y_copy(part, way, d).start()
+                    x_copy(part, way, d, 0).start()
+
+    def second_stage(part, way, d):
+        @pl.when(valid(way, d))
+        def _():
+            y_copy(part, way, d).wait_recv()
+            x_copy(part, way, d, 1).start()
+
+    order = [
+        (part, way, d) for part in range(len(parts)) for d in range(1, n_out) for way in range(2)
+    ]
+    lag = 4
     for step in range(len(order) + lag):
         if step < len(order):
-            cross_inner(*order[step])
+            first_stage(*order[step])
         if step >= lag:
-            cross_rep(*order[step - lag])
-    for item in order:
-        x_copies[item].wait()
-        y_copies[item].wait_send()
-    for copy in z_copies.values():
-        copy.wait_send()
-    for copy in own:
-        copy.wait()
+            second_stage(*order[step - lag])
+    for part, way, d in order:
+
+        @pl.when(valid(way, d))
+        def _():
+            for piece in range(2):
+                x_copy(part, way, d, piece).wait()
+                if d < n_out - 1:
+                    pl.when(onward(way))(lambda: z_copy(part, way, d, piece).wait_send())
+            y_copy(part, way, d).wait_send()
+
+    for part in range(len(parts)):
+        y_own(part).wait()
+        for way in range(2):
+
+            @pl.when(onward(way))
+            def _():
+                z_copy(part, way, 0, 0).wait_send()
+                z_copy(part, way, 0, 1).wait_send()
+
     swap.wait()
 
 
@@ -107,9 +192,15 @@
         full = (rows * members, cols) if rowwise else (rows, cols * members)
         shapes.append(jax.ShapeDtypeStruct(full, shard.dtype))
     shapes.append(jax.ShapeDtypeStruct(resid.shape, resid.dtype))
-    pairs = [(count, n_out - 1)] * 2 + [(count, n_out)] * 4
+    parts = []
+    for w, shard in enumerate(shards):
+        rows = shard.shape[0]
+        pieces = 2 if w >= 4 else 1
+        parts += [(w, piece * (rows // pieces), rows // pieces) for piece in range(pieces)]
+    many = len(parts)
+    pairs = [(many, 2, n_out, 2)] * 2 + [(many, 2, n_out)] * 2 + [(many, 2, n_out, 2)] * 2
     return pl.pallas_call(
-        functools.partial(gather_kernel, by_rows, n_out, n_in),
+        functools.partial(gather_kernel, by_rows, tuple(parts), n_out, n_in),
         out_shape=shapes,
         in_specs=[pl.BlockSpec(memory_space=pltpu.VMEM)] * (count + 1),
         out_specs=[pl.BlockSpec(memory_space=pl.ANY)] * (count + 1),
@@ -255,7 +346,7 @@
     half = jnp.bfloat16
     scale_cols = out_scale.shape[0]
     scales = jnp.concatenate(
-        [jnp.broadcast_to(out_scale, (8, scale_cols)), jnp.broadcast_to(down_scale, (8, scale_cols))]
+        [jnp.broadcast_to(row, (16, scale_cols)) for row in (out_scale, down_scale)]
     )
     shards = [
         v_weight.astype(half),
@@ -268,8 +359,8 @@
     whole_v, whole_u, whole_out, whole_scales, whole_up, whole_down, other = gather_all(
         shards, (True, True, False, True, True, False), resid
     )
-    whole_scales = whole_scales.reshape(-1, 16, scale_cols)
-    out_scales, down_scales = whole_scales[:, 0].reshape(-1), whole_scales[:, 8].reshape(-1)
+    whole_scales = whole_scales.reshape(-1, 32, scale_cols)
+    out_scales, down_scales = whole_scales[:, 0].reshape(-1), whole_scales[:, 16].reshape(-1)
     swap = [(0, 1), (1, 0)]
     full_rows = jnp.where(
         lane == 0,
@@ -377,7 +468,7 @@
         columns = args[9].shape[1] // sizes["fs"]
         depth = args[2].shape[0] // sizes["fs"]
         paired = sizes["rep"] == 2 and sizes["tp"] == 2 and sizes["fs"] % 2 == 0
-        fast = paired and columns % 128 == 0 and depth % 32 == 0
+        fast = paired and columns % 128 == 0 and depth % 128 == 0
         return mapped(local_fast if fast else local)(*args)
 
     def mapped(body):

time: 414 us -> 328 us (0.79)
  Pallas kernels: 303 us -> 217 us
    pallas_call x1, Pallas kernels: 303 us -> 217 us  [gather_all(): pl.pallas_call(functools.partial(gather_kernel, by_rows, tuple(parts), n_...]
where the time goes in v2:
time: 328 us; the launch traced here: 327 us
  Pallas kernels  217 us (66%)
  matrix products  45 us (14%)
  other arithmetic  31.2 us (10%)
  local copies, waits for them, and re-layouts  17.9 us (5%)
  waiting for transfers between devices  10.7 us (3%)
  blocking collectives  4.97 us (2%)
    pallas_call x1, Pallas kernels, gather_all(): pl.pallas_call(functools.partial(gather_kernel, by_rows, tuple(parts), n_...  217 us
    dot_general x1, matrix products, local_fast(): terms = jnp.dot(hidden, whole_down, preferred_element_type=jnp.float32)  25.9 us
    dot_general x1, matrix products, local_fast(): jnp.dot(gated, whole_out, preferred_element_type=jnp.float32)  10.1 us
    reshape x2, local copies, waits for them, and re-layouts, local_fast(): gated = (u_act * mixed.reshape(rows, branch_cols)).astype(jnp.bfloat16)  8.61 us
    reduce_sum x1, other arithmetic, local_fast(): jnp.sum(middle_float * middle_float, axis=1, keepdims=True)  7.37 us
  transfers between devices with their start and end apart: 2, of which 2 were waited for; matrix products, arithmetic and copies ran while one was open for 0% of the time, Pallas kernels for 0%

profile of v2, /device:TPU:0, one launch (start us, length us, event | category | flops | bytes accessed | tf_op | source)
XLA Modules:
  0.0 327.2 jit_solution(1415180377804022923)
XLA Ops:
  0.0 1.2 convert_element_type.67.refs_1_
  1.2 2.0 convert_element_type.66.refs_0_
  3.2 1.8 convert_element_type.68.refs_2_
  5.0 1.7 convert_element_type.69.refs_4_
  7.9 1.2 copy-done.3
  11.0 216.9 %shard_map.172 = (bf16[2048,512]{1,0:T(8,128)(2,1)S(1)}, bf16[2048,512]{1,0:T(8,128)(2,1)S(1)}, bf16[512,2048]{1,0:T(8,128)(2,1)S(1)}, f32[256,256]{1,0:T(8,128)...) custom-call(bf16[256,512]{1,0:T(8,128)(2,1)S(1)} %copy-done.4, ...), custom_call_target="tpu_custom_call" | custom-call | tf_op jit(solution)/shard_map/pallas_call | solution.py:202
  228.0 1.5 fusion.3
  229.5 5.3 %fusion.50 = (f32[1024]{0:T(1024)S(1)}, f32[1024]{0:T(1024)S(1)}, f32[1024,512]{1,0:T(8,128)}) fusion(f32[512]{0:T(512)S(1)} %copy-done.20, bf16[2048,512]{1,0:T(8,128)(2,1)S(1)} %get-tuple-element.14, f32[2048]{0:T(1024)S(1)} %copy-done.17, f32[1024]{0:T(1024)S(1)} %add_rsqrt_fusion.4, bf16[1024,1024]{1,0:T(8,128)(2,1)S(1)} %copy-done, ...), kind=kOutput, calls=%fused_computation.64 | convolution fusion | flops 2181036032 | bytes 8411137 | tf_op jit(solution)/shard_map/dot_general | solution.py:380
  234.9 2.5 all-reduce
  237.4 1.9 multiply_convert_fusion.1
  239.4 2.1 reshape.48
  241.5 3.8 %bitcast_add_fusion = f32[8,128,8,64]{1,3,0,2:T(8,128)} fusion(bf16[8,128,8,64]{3,2,1,0:T(8,128)(2,1)} %reshape.48, f32[128,8]{0,1:T(8,128)S(1)} %bitcast.34, f32[8,128,128]{2,1,0:T(8,128)} %param.25), kind=kOutput, calls=%fused_computation.44 | convolution fusion | flops 134873088 | bytes 3674112 | tf_op jit(solution)/shard_map/gts,bsgd->btgd/dot_general | solution.py:398
  245.2 3.8 %copy.31 = f32[8,128,8,64]{3,2,1,0:T(8,128)} copy(f32[8,128,8,64]{1,3,0,2:T(8,128)} %bitcast_add_fusion) | data formatting | bytes 4194304 | tf_op jit(solution)/shard_map/reshape | solution.py:406
  249.0 4.8 %reshape.49 = f32[1024,512]{1,0:T(8,128)} reshape(f32[8,128,8,64]{3,2,1,0:T(8,128)} %copy.31) | data formatting | bytes 4194304 | tf_op jit(solution)/shard_map/reshape | solution.py:406
  253.9 10.1 %convolution_convert_fusion = bf16[1024,2048]{1,0:T(8,128)(2,1)} fusion(bf16[512,2048]{1,0:T(8,128)(2,1)} %copy-done.9, f32[1024,512]{1,0:T(8,128)} %reshape.49, bf16[2048,512]{1,0:T(8,128)(2,1)} %copy-done.8, f32[2048]{0:T(1024)S(1)} %copy-done.17, f32[1024]{0:T(1024)S(1)} %add_rsqrt_fusion.4, f32[512]{0:T(512)S(1)} %copy-done.21, ...), kind=kOutput, calls=%fused_computation.24 | convolution fusion | flops 4330094592 | bytes 14694401 | tf_op jit(solution)/shard_map/dot_general | solution.py:407
  265.0 6.5 %collective-permute-done = bf16[1024,2048]{1,0:T(8,128)(2,1)} collective-permute-done((bf16[1024,2048]{1,0:T(8,128)(2,1)}, bf16[1024,2048]{1,0:T(8,128)(2,1)}, u32[]{:S(2)}, u32[]{:S(2)}) %collective-permute-start) | collective-permute-done | bytes 4194336 | tf_op jit(solution)/shard_map/ppermute | solution.py:414
  271.4 5.3 %multiply_reduce_fusion = f32[1024]{0:T(1024)S(1)} fusion(bf16[1024,2048]{1,0:T(8,128)(2,1)} %collective-permute-done, bf16[1024,2048]{1,0:T(8,128)(2,1)} %convolution_convert_fusion, f32[2048]{0:T(1024)S(1)} %bitcast.25), kind=kLoop, calls=%fused_computation.13 | loop fusion | flops 12581888 | bytes 8400896 | tf_op jit(solution)/shard_map/reduce_sum | solution.py:416
  276.8 7.4 %fusion = (f32[1024]{0:T(1024)S(1)}, bf16[1024,2048]{1,0:T(8,128)(2,1)}) fusion(f32[2048]{0:T(1024)S(1)} %copy-done.12, f32[1024]{0:T(1024)S(1)} %add_rsqrt_fusion.2, f32[2048]{0:T(1024)S(1)} %bitcast.26, bf16[1024,2048]{1,0:T(8,128)(2,1)} %collective-permute-done, bf16[1024,2048]{1,0:T(8,128)(2,1)S(1)} %copy-done.10, bf16[1024,1024]{1,0:T(8,128)(2,1)S(1)} %copy-done, ...), kind=kLoop, calls=%fused_computation.5 | loop fusion | flops 44039168 | bytes 16801792 | tf_op jit(solution)/shard_map/reduce_sum | solution.py:424
  284.2 25.9 %fusion.16 = bf16[1024,2048]{1,0:T(8,128)(2,1)} fusion(bf16[2048,2048]{1,0:T(8,128)(2,1)} %get-tuple-element.18, bf16[2048,2048]{1,0:T(8,128)(2,1)} %copy-done.7, bf16[1024,2048]{1,0:T(8,128)(2,1)} %get-tuple-element.24, f32[2048]{0:T(1024)S(1)} %copy-done.18, f32[2048]{0:T(1024)S(1)} %copy-done.19, f32[1024]{0:T(1024)S(1)} %add_rsqrt_fusion.1), kind=kOutput, calls=%fused_computation.25 | convolution fusion | flops 17198743552 | bytes 25186304 | tf_op jit(solution)/shard_map/dot_general | solution.py:428
  310.1 3.1 constant_dynamic-slice_fusion
  313.3 4.2 %collective-permute-done.1 = bf16[1024,1024]{1,0:T(8,128)(2,1)S(1)} collective-permute-done((bf16[1024,1024]{1,0:T(8,128)(2,1)}, bf16[1024,1024]{1,0:T(8,128)(2,1)S(1)}, u32[]{:S(2)}, u32[]{:S(2)}) %collective-permute-start.1) | collective-permute-done | bytes 2097184 | tf_op jit(solution)/shard_map/ppermute | solution.py:434
  317.5 2.5 multiply_reduce_fusion.1
  320.0 2.5 psum.23
  322.5 4.7 %add_convert_fusion = bf16[1024,1024]{1,0:T(8,128)(2,1)} fusion(bf16[1024,1024]{1,0:T(8,128)(2,1)S(1)} %collective-permute-done.1, f32[1024]{0:T(1024)S(1)} %dynamic-slice-done, f32[1024]{0:T(1024)S(1)} %bitcast.28, f32[1024]{0:T(1024)S(1)} %dynamic_slice.18, bf16[1024,2048]{1,0:T(8,128)(2,1)} %get-tuple-element.24, s32[]{:T(128)} %select_n.19, ...), kind=kLoop, calls=%fused_computation.17 | loop fusion | flops 9437184 | bytes 8400900 | tf_op jit(solution)/shard_map/convert_element_type | solution.py:438
  (58 shorter events, 4.3 us)
Async XLA Ops:
  0.0 6.7 %copy-start.11 = (f32[2048,256]{1,0:T(8,128)S(1)}, f32[2048,256]{1,0:T(8,128)}, u32[]{:S(2)}) copy-start(f32[2048,256]{1,0:T(8,128)} %param.33) | copy-start | bytes 6291460
  0.0 7.8 %copy-start.15 = (f32[256]{0:T(256)S(1)}, f32[256]{0:T(256)}, u32[]{:S(2)}) copy-start(f32[256]{0:T(256)} %param.28) | copy-start | bytes 3076
  0.0 7.8 %copy-start.16 = (f32[256]{0:T(256)S(1)}, f32[256]{0:T(256)}, u32[]{:S(2)}) copy-start(f32[256]{0:T(256)} %param.34) | copy-start | bytes 3076
  0.0 7.8 %copy-start = (bf16[1024,1024]{1,0:T(8,128)(2,1)S(1)}, bf16[1024,1024]{1,0:T(8,128)(2,1)}, u32[]{:S(2)}) copy-start(bf16[1024,1024]{1,0:T(8,128)(2,1)} %refs_6_.1) | copy-start | bytes 6291460
  7.9 1.2 copy-start.3
  9.1 0.9 copy-start.4
  11.0 218.5 %copy-start.17 = (f32[2048]{0:T(1024)S(1)}, f32[2048]{0:T(1024)}, u32[]{:S(2)}) copy-start(f32[2048]{0:T(1024)} %param.19) | copy-start | bytes 24580
  11.0 218.5 %copy-start.20 = (f32[512]{0:T(512)S(1)}, f32[512]{0:T(512)}, u32[]{:S(2)}) copy-start(f32[512]{0:T(512)} %param.23) | copy-start | bytes 6148
  227.9 6.9 %copy-start.1 = (bf16[1024,1024]{1,0:T(8,128)(2,1)}, bf16[1024,1024]{1,0:T(8,128)(2,1)S(1)}, u32[]{:S(2)}) copy-start(bf16[1024,1024]{1,0:T(8,128)(2,1)S(1)} %get-tuple-element.12) | copy-start | bytes 6291460
  227.9 6.9 %copy-start.6 = (f32[256,256]{1,0:T(8,128)}, f32[256,256]{1,0:T(8,128)S(1)}, u32[]{:S(2)}) copy-start(f32[256,256]{1,0:T(8,128)S(1)} %get-tuple-element.16) | copy-start | bytes 786436
  227.9 6.9 %copy-start.7 = (bf16[2048,2048]{1,0:T(8,128)(2,1)}, bf16[2048,2048]{1,0:T(8,128)(2,1)S(1)}, u32[]{:S(2)}) copy-start(bf16[2048,2048]{1,0:T(8,128)(2,1)S(1)} %get-tuple-element.17) | copy-start | bytes 25165828
  227.9 6.9 %copy-start.8 = (bf16[2048,512]{1,0:T(8,128)(2,1)}, bf16[2048,512]{1,0:T(8,128)(2,1)S(1)}, u32[]{:S(2)}) copy-start(bf16[2048,512]{1,0:T(8,128)(2,1)S(1)} %get-tuple-element.13) | copy-start | bytes 6291460
  228.0 6.9 %copy-start.9 = (bf16[512,2048]{1,0:T(8,128)(2,1)}, bf16[512,2048]{1,0:T(8,128)(2,1)S(1)}, u32[]{:S(2)}) copy-start(bf16[512,2048]{1,0:T(8,128)(2,1)S(1)} %get-tuple-element.15) | copy-start | bytes 6291460
  229.5 7.9 %copy-start.14 = (f32[512]{0:T(512)S(1)}, f32[512]{0:T(512)}, u32[]{:S(2)}) copy-start(f32[512]{0:T(512)} %param.24) | copy-start | bytes 6148
  234.9 6.6 %copy-start.13 = (f32[8,128]{1,0:T(8,128)S(1)}, f32[8,128]{1,0:T(8,128)}, u32[]{:S(2)}) copy-start(f32[8,128]{1,0:T(8,128)} %param.26) | copy-start | bytes 12292
  249.0 4.8 %copy-start.21 = (f32[512]{0:T(512)S(1)}, f32[512]{0:T(512)}, u32[]{:S(2)}) copy-start(f32[512]{0:T(512)} %param.22) | copy-start | bytes 6148
  263.9 7.5 %collective-permute-start = (bf16[1024,2048]{1,0:T(8,128)(2,1)}, bf16[1024,2048]{1,0:T(8,128)(2,1)}, u32[]{:S(2)}, u32[]{:S(2)}) collective-permute-start(bf16[1024,2048]{1,0:T(8,128)(2,1)} %convolution_convert_fusion), channel_id=1, source_target_pairs={{0,1},{1,0},{2,3},{3,2},{4,5},{5,4},{6,7},{7,6},{8,9},{9,8},{10,11... | collective-permute-start | bytes 12582920 | tf_op jit(solution)/shard_map/ppermute | solution.py:414
  271.4 5.3 %copy-start.2 = (bf16[1024,1024]{1,0:T(8,128)(2,1)S(1)}, bf16[1024,1024]{1,0:T(8,128)(2,1)}, u32[]{:S(2)}) copy-start(bf16[1024,1024]{1,0:T(8,128)(2,1)} %copy-done.1) | copy-start | bytes 6291460
  271.4 5.3 %copy-start.10 = (bf16[1024,2048]{1,0:T(8,128)(2,1)S(1)}, bf16[1024,2048]{1,0:T(8,128)(2,1)}, u32[]{:S(2)}) copy-start(bf16[1024,2048]{1,0:T(8,128)(2,1)} %convolution_convert_fusion) | copy-start | bytes 12582916
  271.4 5.3 %copy-start.12 = (f32[2048]{0:T(1024)S(1)}, f32[2048]{0:T(1024)}, u32[]{:S(2)}) copy-start(f32[2048]{0:T(1024)} %param.29) | copy-start | bytes 24580
  276.8 7.4 %copy-start.18 = (f32[2048]{0:T(1024)S(1)}, f32[2048]{0:T(1024)}, u32[]{:S(2)}) copy-start(f32[2048]{0:T(1024)} %param.32) | copy-start | bytes 24580
  276.8 7.4 %copy-start.19 = (f32[2048]{0:T(1024)S(1)}, f32[2048]{0:T(1024)}, u32[]{:S(2)}) copy-start(f32[2048]{0:T(1024)} %param.30) | copy-start | bytes 24580
  313.2 4.4 %collective-permute-start.1 = (bf16[1024,1024]{1,0:T(8,128)(2,1)}, bf16[1024,1024]{1,0:T(8,128)(2,1)S(1)}, u32[]{:S(2)}, u32[]{:S(2)}) collective-permute-start(bf16[1024,1024]{1,0:T(8,128)(2,1)} %constant_dynamic-slice_fusion), channel_id=1, source_target_pairs={{0,1},{1,0},{2,3},{3,2},{4,5},{5,4},{6,7},{7,6},{8,9},{9,8},{10,11... | collective-permute-start | bytes 6291464 | tf_op jit(solution)/shard_map/ppermute | solution.py:434
  313.3 9.2 %dynamic-slice-start = ((f32[2048]{0:T(1024)}, s32[]{:T(128)}), f32[1024]{0:T(1024)S(1)}, s32[]{:S(2)}) async-start(f32[2048]{0:T(1024)} %param.35, s32[]{:T(128)} %select_n.19), calls=%async_computation | async-start | bytes 8704 | tf_op jit(solution)/shard_map/dynamic_slice | solution.py:437
  (1 other events, 0.9 us)

commit v3 on v2

--- a/solution.py
+++ b/solution.py
@@ -354,10 +354,10 @@
         out_weight.astype(half),
         scales,
         up_weight.astype(half),
-        down_weight.astype(half),
     ]
-    whole_v, whole_u, whole_out, whole_scales, whole_up, whole_down, other = gather_all(
-        shards, (True, True, False, True, True, False), resid
+    whole_down = lax.all_gather(down_weight.astype(half), "fs", axis=1, tiled=True)
+    whole_v, whole_u, whole_out, whole_scales, whole_up, other = gather_all(
+        shards, (True, True, False, True, True), resid
     )
     whole_scales = whole_scales.reshape(-1, 32, scale_cols)
     out_scales, down_scales = whole_scales[:, 0].reshape(-1), whole_scales[:, 16].reshape(-1)

time: 328 us -> 340 us (1.037)
  between operations: 0.27 us -> 13.7 us
  transfers between devices with their start and end apart: 2 -> 3, of which waited for: 2 -> 2; matrix products, arithmetic and copies ran while one was open for 0% -> 15% of each run, Pallas kernels for 0% -> 64%
where the time goes in v3:
time: 340 us; the launch traced here: 338 us
  Pallas kernels  216 us (64%)
  matrix products  45 us (13%)
  other arithmetic  30.5 us (9%)
  local copies, waits for them, and re-layouts  16.7 us (5%)
  between operations  13.7 us (4%)
  waiting for transfers between devices  10.7 us (3%)
  blocking collectives  4.97 us (1%)
    pallas_call x1, Pallas kernels, gather_all(): pl.pallas_call(functools.partial(gather_kernel, by_rows, tuple(parts), n_...  216 us
    dot_general x1, matrix products, local_fast(): terms = jnp.dot(hidden, whole_down, preferred_element_type=jnp.float32)  25.9 us
    dot_general x1, matrix products, local_fast(): jnp.dot(gated, whole_out, preferred_element_type=jnp.float32)  10.1 us
    reshape x2, local copies, waits for them, and re-layouts, local_fast(): gated = (u_act * mixed.reshape(rows, branch_cols)).astype(jnp.bfloat16)  8.63 us
    reduce_sum x1, other arithmetic, local_fast(): jnp.sum(middle_float * middle_float, axis=1, keepdims=True)  7.35 us
  transfers between devices with their start and end apart: 3, of which 2 were waited for; matrix products, arithmetic and copies ran while one was open for 15% of the time, Pallas kernels for 64%

profile of v3, /device:TPU:0, one launch (start us, length us, event | category | flops | bytes accessed | tf_op | source)
XLA Modules:
  0.0 337.9 jit_solution(3825286051420634295)
XLA Ops:
  6.5 2.8 convert_element_type.83
  9.4 1.8 convert_element_type.69.refs_4_
  11.2 1.1 convert_element_type.66.refs_0_
  13.9 0.9 copy-done.3
  14.8 0.9 copy-done.4
  15.8 216.0 %shard_map.172 = (bf16[2048,512]{1,0:T(8,128)(2,1)S(1)}, bf16[2048,512]{1,0:T(8,128)(2,1)S(1)}, bf16[512,2048]{1,0:T(8,128)(2,1)S(1)}, f32[256,256]{1,0:T(8,128)...) custom-call(bf16[256,512]{1,0:T(8,128)(2,1)S(1)} %convert_element_type.66.refs_0_, ...), custom_call_target="tpu_custom_call" | custom-call | tf_op jit(solution)/shard_map/pallas_call | solution.py:202
  231.8 1.5 fusion.3
  233.4 5.3 %fusion.50 = (f32[1024]{0:T(1024)S(1)}, f32[1024]{0:T(1024)S(1)}, f32[1024,512]{1,0:T(8,128)}) fusion(f32[512]{0:T(512)S(1)} %copy-done.20, bf16[2048,512]{1,0:T(8,128)(2,1)S(1)} %get-tuple-element.13, f32[2048]{0:T(1024)S(1)} %copy-done.17, f32[1024]{0:T(1024)S(1)} %add_rsqrt_fusion.4, bf16[1024,1024]{1,0:T(8,128)(2,1)S(1)} %copy-done, ...), kind=kOutput, calls=%fused_computation.64 | convolution fusion | flops 2181036032 | bytes 8411137 | tf_op jit(solution)/shard_map/dot_general | solution.py:380
  238.7 2.5 all-reduce
  241.3 1.9 multiply_convert_fusion.1
  243.2 2.1 reshape.48
  245.3 3.7 %bitcast_add_fusion = f32[8,128,8,64]{1,3,0,2:T(8,128)} fusion(bf16[8,128,8,64]{3,2,1,0:T(8,128)(2,1)} %reshape.48, f32[128,8]{0,1:T(8,128)S(1)} %bitcast.34, f32[8,128,128]{2,1,0:T(8,128)} %param.25), kind=kOutput, calls=%fused_computation.44 | convolution fusion | flops 134873088 | bytes 3674112 | tf_op jit(solution)/shard_map/gts,bsgd->btgd/dot_general | solution.py:398
  249.1 3.8 %copy.31 = f32[8,128,8,64]{3,2,1,0:T(8,128)} copy(f32[8,128,8,64]{1,3,0,2:T(8,128)} %bitcast_add_fusion) | data formatting | bytes 4194304 | tf_op jit(solution)/shard_map/reshape | solution.py:406
  252.9 4.8 %reshape.49 = f32[1024,512]{1,0:T(8,128)} reshape(f32[8,128,8,64]{3,2,1,0:T(8,128)} %copy.31) | data formatting | bytes 4194304 | tf_op jit(solution)/shard_map/reshape | solution.py:406
  257.7 10.1 %convolution_convert_fusion = bf16[1024,2048]{1,0:T(8,128)(2,1)} fusion(bf16[512,2048]{1,0:T(8,128)(2,1)} %copy-done.8, f32[1024,512]{1,0:T(8,128)} %reshape.49, bf16[2048,512]{1,0:T(8,128)(2,1)} %copy-done.7, f32[2048]{0:T(1024)S(1)} %copy-done.17, f32[1024]{0:T(1024)S(1)} %add_rsqrt_fusion.4, f32[512]{0:T(512)S(1)} %copy-done.21, ...), kind=kOutput, calls=%fused_computation.24 | convolution fusion | flops 4330094592 | bytes 14694401 | tf_op jit(solution)/shard_map/dot_general | solution.py:407
  268.8 6.5 %collective-permute-done = bf16[1024,2048]{1,0:T(8,128)(2,1)} collective-permute-done((bf16[1024,2048]{1,0:T(8,128)(2,1)}, bf16[1024,2048]{1,0:T(8,128)(2,1)}, u32[]{:S(2)}, u32[]{:S(2)}) %collective-permute-start) | collective-permute-done | bytes 4194336 | tf_op jit(solution)/shard_map/ppermute | solution.py:414
  275.3 5.3 %multiply_reduce_fusion = f32[1024]{0:T(1024)S(1)} fusion(bf16[1024,2048]{1,0:T(8,128)(2,1)} %collective-permute-done, bf16[1024,2048]{1,0:T(8,128)(2,1)} %convolution_convert_fusion, f32[2048]{0:T(1024)S(1)} %bitcast.25), kind=kLoop, calls=%fused_computation.13 | loop fusion | flops 12581888 | bytes 8400896 | tf_op jit(solution)/shard_map/reduce_sum | solution.py:416
  280.6 7.4 %fusion = (f32[1024]{0:T(1024)S(1)}, bf16[1024,2048]{1,0:T(8,128)(2,1)}) fusion(f32[2048]{0:T(1024)S(1)} %copy-done.12, f32[1024]{0:T(1024)S(1)} %add_rsqrt_fusion.2, f32[2048]{0:T(1024)S(1)} %bitcast.26, bf16[1024,2048]{1,0:T(8,128)(2,1)} %collective-permute-done, bf16[1024,2048]{1,0:T(8,128)(2,1)S(1)} %copy-done.9, bf16[1024,1024]{1,0:T(8,128)(2,1)S(1)} %copy-done, ...), kind=kLoop, calls=%fused_computation.5 | loop fusion | flops 44039168 | bytes 16801792 | tf_op jit(solution)/shard_map/reduce_sum | solution.py:424
  288.0 25.9 %fusion.16 = bf16[1024,2048]{1,0:T(8,128)(2,1)} fusion(bf16[2048,2048]{1,0:T(8,128)(2,1)} %all-gather.2.cloned.1.call-done, bf16[2048,2048]{1,0:T(8,128)(2,1)} %copy-done.6, bf16[1024,2048]{1,0:T(8,128)(2,1)} %get-tuple-element.22, f32[2048]{0:T(1024)S(1)} %copy-done.18, f32[2048]{0:T(1024)S(1)} %copy-done.19, f32[1024]{0:T(1024)S(1)} %add_rsqrt_fusion.1), kind=kOutput, calls=%fused_computation.25 | convolution fusion | flops 17198743552 | bytes 25186304 | tf_op jit(solution)/shard_map/dot_general | solution.py:428
  313.9 3.1 constant_dynamic-slice_fusion
  317.1 4.2 %collective-permute-done.1 = bf16[1024,1024]{1,0:T(8,128)(2,1)S(1)} collective-permute-done((bf16[1024,1024]{1,0:T(8,128)(2,1)}, bf16[1024,1024]{1,0:T(8,128)(2,1)S(1)}, u32[]{:S(2)}, u32[]{:S(2)}) %collective-permute-start.1) | collective-permute-done | bytes 2097184 | tf_op jit(solution)/shard_map/ppermute | solution.py:434
  321.4 2.5 multiply_reduce_fusion.1
  323.8 2.5 psum.23
  326.3 4.7 %add_convert_fusion = bf16[1024,1024]{1,0:T(8,128)(2,1)} fusion(bf16[1024,1024]{1,0:T(8,128)(2,1)S(1)} %collective-permute-done.1, f32[1024]{0:T(1024)S(1)} %dynamic-slice-done, f32[1024]{0:T(1024)S(1)} %bitcast.28, f32[1024]{0:T(1024)S(1)} %dynamic_slice.18, bf16[1024,2048]{1,0:T(8,128)(2,1)} %get-tuple-element.22, s32[]{:T(128)} %select_n.19, ...), kind=kLoop, calls=%fused_computation.17 | loop fusion | flops 9437184 | bytes 8400900 | tf_op jit(solution)/shard_map/convert_element_type | solution.py:438
  (61 shorter events, 2.9 us)
Async XLA Ops:
  6.5 7.3 %copy-start.15 = (f32[256]{0:T(256)S(1)}, f32[256]{0:T(256)}, u32[]{:S(2)}) copy-start(f32[256]{0:T(256)} %param.28) | copy-start | bytes 3076
  6.5 7.3 %copy-start.16 = (f32[256]{0:T(256)S(1)}, f32[256]{0:T(256)}, u32[]{:S(2)}) copy-start(f32[256]{0:T(256)} %param.34) | copy-start | bytes 3076
  6.5 7.3 %copy-start = (bf16[1024,1024]{1,0:T(8,128)(2,1)S(1)}, bf16[1024,1024]{1,0:T(8,128)(2,1)}, u32[]{:S(2)}) copy-start(bf16[1024,1024]{1,0:T(8,128)(2,1)} %refs_5_.1) | copy-start | bytes 6291460
  6.5 281.4 %all-gather.2.cloned.1.call-start = ((), (), s32[]{:S(2)}) async-start(), calls=%async_computation | async-start | bytes 9437184 | tf_op jit(solution)/shard_map/all_gather | solution.py:358
  9.4 2.9 copy-start.10
  9.4 3.7 %copy-start.11 = (f32[512,256]{1,0:T(8,128)S(1)}, f32[512,256]{1,0:T(8,128)}, u32[]{:S(2)}) copy-start(f32[512,256]{1,0:T(8,128)} %param.27) | copy-start | bytes 1572868
  13.8 219.5 %copy-start.17 = (f32[2048]{0:T(1024)S(1)}, f32[2048]{0:T(1024)}, u32[]{:S(2)}) copy-start(f32[2048]{0:T(1024)} %param.19) | copy-start | bytes 24580
  13.8 219.5 %copy-start.20 = (f32[512]{0:T(512)S(1)}, f32[512]{0:T(512)}, u32[]{:S(2)}) copy-start(f32[512]{0:T(512)} %param.23) | copy-start | bytes 6148
  231.8 6.9 %copy-start.1 = (bf16[1024,1024]{1,0:T(8,128)(2,1)}, bf16[1024,1024]{1,0:T(8,128)(2,1)S(1)}, u32[]{:S(2)}) copy-start(bf16[1024,1024]{1,0:T(8,128)(2,1)S(1)} %get-tuple-element.11) | copy-start | bytes 6291460
  231.8 6.9 %copy-start.5 = (f32[256,256]{1,0:T(8,128)}, f32[256,256]{1,0:T(8,128)S(1)}, u32[]{:S(2)}) copy-start(f32[256,256]{1,0:T(8,128)S(1)} %get-tuple-element.15) | copy-start | bytes 786436
  231.8 6.9 %copy-start.6 = (bf16[2048,2048]{1,0:T(8,128)(2,1)}, bf16[2048,2048]{1,0:T(8,128)(2,1)S(1)}, u32[]{:S(2)}) copy-start(bf16[2048,2048]{1,0:T(8,128)(2,1)S(1)} %get-tuple-element.16) | copy-start | bytes 25165828
  231.8 6.9 %copy-start.7 = (bf16[2048,512]{1,0:T(8,128)(2,1)}, bf16[2048,512]{1,0:T(8,128)(2,1)S(1)}, u32[]{:S(2)}) copy-start(bf16[2048,512]{1,0:T(8,128)(2,1)S(1)} %get-tuple-element.12) | copy-start | bytes 6291460
  231.8 6.9 %copy-start.8 = (bf16[512,2048]{1,0:T(8,128)(2,1)}, bf16[512,2048]{1,0:T(8,128)(2,1)S(1)}, u32[]{:S(2)}) copy-start(bf16[512,2048]{1,0:T(8,128)(2,1)S(1)} %get-tuple-element.14) | copy-start | bytes 6291460
  233.4 7.9 %copy-start.14 = (f32[512]{0:T(512)S(1)}, f32[512]{0:T(512)}, u32[]{:S(2)}) copy-start(f32[512]{0:T(512)} %param.24) | copy-start | bytes 6148
  238.7 6.6 %copy-start.13 = (f32[8,128]{1,0:T(8,128)S(1)}, f32[8,128]{1,0:T(8,128)}, u32[]{:S(2)}) copy-start(f32[8,128]{1,0:T(8,128)} %param.26) | copy-start | bytes 12292
  252.9 4.8 %copy-start.21 = (f32[512]{0:T(512)S(1)}, f32[512]{0:T(512)}, u32[]{:S(2)}) copy-start(f32[512]{0:T(512)} %param.22) | copy-start | bytes 6148
  267.8 7.5 %collective-permute-start = (bf16[1024,2048]{1,0:T(8,128)(2,1)}, bf16[1024,2048]{1,0:T(8,128)(2,1)}, u32[]{:S(2)}, u32[]{:S(2)}) collective-permute-start(bf16[1024,2048]{1,0:T(8,128)(2,1)} %convolution_convert_fusion), channel_id=1, source_target_pairs={{0,1},{1,0},{2,3},{3,2},{4,5},{5,4},{6,7},{7,6},{8,9},{9,8},{10,11... | collective-permute-start | bytes 12582920 | tf_op jit(solution)/shard_map/ppermute | solution.py:414
  275.3 5.3 %copy-start.2 = (bf16[1024,1024]{1,0:T(8,128)(2,1)S(1)}, bf16[1024,1024]{1,0:T(8,128)(2,1)}, u32[]{:S(2)}) copy-start(bf16[1024,1024]{1,0:T(8,128)(2,1)} %copy-done.1) | copy-start | bytes 6291460
  275.3 5.3 %copy-start.9 = (bf16[1024,2048]{1,0:T(8,128)(2,1)S(1)}, bf16[1024,2048]{1,0:T(8,128)(2,1)}, u32[]{:S(2)}) copy-start(bf16[1024,2048]{1,0:T(8,128)(2,1)} %convolution_convert_fusion) | copy-start | bytes 12582916
  275.3 5.3 %copy-start.12 = (f32[2048]{0:T(1024)S(1)}, f32[2048]{0:T(1024)}, u32[]{:S(2)}) copy-start(f32[2048]{0:T(1024)} %param.29) | copy-start | bytes 24580
  280.6 7.4 %copy-start.18 = (f32[2048]{0:T(1024)S(1)}, f32[2048]{0:T(1024)}, u32[]{:S(2)}) copy-start(f32[2048]{0:T(1024)} %param.32) | copy-start | bytes 24580
  280.6 7.4 %copy-start.19 = (f32[2048]{0:T(1024)S(1)}, f32[2048]{0:T(1024)}, u32[]{:S(2)}) copy-start(f32[2048]{0:T(1024)} %param.30) | copy-start | bytes 24580
  317.0 4.4 %collective-permute-start.1 = (bf16[1024,1024]{1,0:T(8,128)(2,1)}, bf16[1024,1024]{1,0:T(8,128)(2,1)S(1)}, u32[]{:S(2)}, u32[]{:S(2)}) collective-permute-start(bf16[1024,1024]{1,0:T(8,128)(2,1)} %constant_dynamic-slice_fusion), channel_id=1, source_target_pairs={{0,1},{1,0},{2,3},{3,2},{4,5},{5,4},{6,7},{7,6},{8,9},{9,8},{10,11... | collective-permute-start | bytes 6291464 | tf_op jit(solution)/shard_map/ppermute | solution.py:434
  317.1 9.2 %dynamic-slice-start = ((f32[2048]{0:T(1024)}, s32[]{:T(128)}), f32[1024]{0:T(1024)S(1)}, s32[]{:S(2)}) async-start(f32[2048]{0:T(1024)} %param.35, s32[]{:T(128)} %select_n.19), calls=%async_computation.1 | async-start | bytes 8704 | tf_op jit(solution)/shard_map/dynamic_slice | solution.py:437
  (2 other events, 1.9 us)
Sparse Core Ops, SparseCore 0:
  9.5 201.2 all-gather.1
